TPU v7x, 512 devices: a whole 4x8x8 slice. The times are simulated.
512 devices in a mesh: sp: 32 (over z, x), tp: 16 (over y, core).
Axes of the slice: x: 4, y: 8, z: 8, core: 2. Of those that a mesh axis runs over, the one named last changes fastest.
Arguments:
- ffn_input: bfloat16 [4096, 2048], P('sp', 'tp'), may hold values from -6 to 6
- out_grad: bfloat16 [4096, 2048], P('sp', 'tp'), may hold values from -6 to 6
- routes: int32 [4096, 2], P('sp'), may hold values from 0 to 31, all different within a row; in each aligned block of 128 rows (0 to 127, 128 to 255, ...) at most 10 rows name the same one
- route_weight: float32 [4096, 2], P('sp'), may hold values from 0.05 to 1
- gate_w: bfloat16 [32, 2048, 2048], P('sp', None, 'tp'), may hold values from -0.125 to 0.125
- up_w: bfloat16 [32, 2048, 2048], P('sp', None, 'tp'), may hold values from -0.125 to 0.125
- down_w: bfloat16 [32, 2048, 2048], P('sp', 'tp'), may hold values from -0.125 to 0.125
- out_proj: bfloat16 [2048, 2048], P('tp'), may hold values from -0.125 to 0.125
- rec_value: bfloat16 [4096, 2048], P('sp', 'tp'), may hold values from -6 to 6
- rate_pre: bfloat16 [4096, 2048], P('sp', 'tp'), may hold values from -6 to 6
- input_pre: bfloat16 [4096, 2048], P('sp', 'tp'), may hold values from -4 to 4
- prev_state: bfloat16 [4096, 2048], P('sp', 'tp'), may hold values from -6 to 6
- decay_param: float32 [2048], P('tp'), may hold values from 4 to 12
Outputs:
- gate_w_grad: bfloat16 [32, 2048, 2048], P('sp', None, 'tp')
- up_w_grad: bfloat16 [32, 2048, 2048], P('sp', None, 'tp')
- down_w_grad: bfloat16 [32, 2048, 2048], P('sp', 'tp')
- out_proj_grad: float32 [2048, 2048], P('sp', 'tp')
- rec_value_grad: bfloat16 [4096, 2048], P('sp', 'tp')
- rate_pre_grad: bfloat16 [4096, 2048], P('sp', 'tp')
- input_pre_grad: bfloat16 [4096, 2048], P('sp', 'tp')
Inputs may be any that keep to these rules, and one draw needn't show every extreme that they name: `routes`: each token names 2 different experts. Within each aligned block of 128 tokens no expert is named more than 10 times, a bound that some block reaches.
All inputs are finite; a program needn't handle non-finite values.
Results may differ from a plain program's by a relative error of at most 0.02.
Values may be sent and summed in bfloat16 or wider, within the bound.
No kernel may reach another device: no remote copies, remote signals or barrier semaphores. Data moves between devices by JAX's collectives and lax.ppermute only.
A program may use at most 64 MiB of HBM per device.

v0:
```python
import jax
import jax.numpy as jnp
from jax import lax
from jax.sharding import Mesh
from jax.sharding import PartitionSpec as P

SP = ("sp_0", "sp_1")


decay_scale = 8.0


def in_one_piece(arrays, axis, split_dim, concat_dim, along):
    both = jnp.concatenate(arrays, axis=along)
    filled, at, finished = (
        lax.all_to_all(both, axis, split_axis=split_dim, concat_axis=concat_dim, tiled=True),
        0,
        [],
    )
    for a in arrays:
        finished.append(lax.slice_in_dim(filled, at, at + a.shape[along], axis=along))
        at += a.shape[along]
    return tuple(finished)


def sent_together(arrays, axis, dim, along):
    ends, at = ([], 0)
    for a in arrays[:-1]:
        at += a.shape[along]
        ends.append(at)
    both = jnp.concatenate(arrays, axis=along)
    return tuple(jnp.split(lax.all_gather(both, axis, axis=dim, tiled=True), ends, axis=along))


def split_up(shard, dim, length):
    lengths = shard.shape
    tiles = shard.reshape(*lengths[:dim], length, lengths[dim] // length, *lengths[dim + 1 :])
    return jnp.moveaxis(tiles, dim, 0)


def sent_and_summed(shard, axis, dim):
    tiles = split_up(shard, dim, lax.axis_size(axis))
    arrived = lax.all_to_all(tiles, axis, split_axis=0, concat_axis=0, tiled=True)
    return arrived.astype(jnp.float32).sum(axis=0)


def neutral_like(shard, identity):
    return jax.tree.map(
        lambda a, e: jnp.broadcast_to(jnp.asarray(e, a.dtype), a.shape), shard, identity
    )


def all_in_one(shard, axis):
    leaves = jax.tree.leaves(shard)
    sequence = sorted(range(len(leaves)), key=lambda k: -leaves[k].size)
    width = (1, *leaves[sequence[0]].shape)[-1]
    lines = [
        jnp.pad(leaves[k].reshape(-1), (0, -leaves[k].size % width)).reshape(-1, width)
        for k in sequence
    ]
    both, at, found = (lax.all_gather(jnp.concatenate(lines), axis), 0, {})
    for k, line in zip(sequence, lines):
        share = both[:, at : at + len(line)].reshape(len(both), -1)
        found[k] = share[:, : leaves[k].size].reshape(-1, *leaves[k].shape)
        at += len(line)
    numbers = iter(range(len(leaves)))
    return jax.tree.map(lambda _: found[next(numbers)], shard)


def entering(shard, axes, combine, identity):
    before = start = neutral_like(shard, identity)
    so_far = shard
    for axis in reversed(axes):
        length, here = (lax.axis_size(axis), lax.axis_index(axis))
        pieces = all_in_one(so_far, axis)
        inside, so_far = (start, start)
        for k in reversed(range(length)):
            passed = k > here
            so_far = combine(so_far, jax.tree.map(lambda part: part[k], pieces))
            inside = jax.tree.map(lambda new, old: jnp.where(passed, new, old), so_far, inside)
        before = combine(inside, before)
    return before


def chain_link(left_pair, right_pair):
    return (left_pair[0] * right_pair[0], right_pair[0] * left_pair[1] + right_pair[1])


def compose(earlier_map, later_map):
    return (later_map[0] * earlier_map[0], later_map[1] + later_map[0] * earlier_map[1])


def slot_layout(routes, experts, capacity):
    flat_routes = routes.reshape(-1)
    route_marks = (flat_routes[:, None] == jnp.arange(experts, dtype=jnp.int32)[None, :]).astype(
        jnp.int32
    )
    before = jnp.sum((jnp.cumsum(route_marks, axis=0) - route_marks) * route_marks, axis=1)
    slot_index = flat_routes * capacity + before
    slot_total = experts * capacity
    route_ids = jnp.arange(flat_routes.shape[0], dtype=jnp.int32)
    slot_owner = jnp.zeros((slot_total,), jnp.int32).at[slot_index].set(route_ids)
    filled = jnp.zeros((slot_total,), jnp.int32).at[slot_index].set(1)
    return (slot_index, slot_owner, filled)


def fill_slots(tokens_in, cotangent, route_weight, slot_owner, filled, route_count):
    token_index = slot_owner // route_count
    kept_mask = filled[:, None] > 0
    rows_in = jnp.where(
        kept_mask, jnp.take(tokens_in, token_index, axis=0), jnp.zeros((), jnp.bfloat16)
    )
    weights = route_weight.reshape(-1)[slot_owner][:, None]
    scaled = (weights * jnp.take(cotangent, token_index, axis=0).astype(jnp.float32)).astype(
        jnp.bfloat16
    )
    rows_cot = jnp.where(kept_mask, scaled, jnp.zeros((), jnp.bfloat16))
    return (rows_in, rows_cot)


def expert_work(rows_in, rows_cot, w_gate, w_up, w_down):
    across = (((0,), (0,)), ((), ()))
    inner = (((1,), (1,)), ((), ()))
    gate_act = jnp.dot(rows_in, w_gate, preferred_element_type=jnp.float32)
    up_act = jnp.dot(rows_in, w_up, preferred_element_type=jnp.float32)
    squash = jax.nn.sigmoid(gate_act)
    silu_gate = gate_act * squash
    hidden = (silu_gate * up_act).astype(jnp.bfloat16)
    down_grad = lax.dot_general(
        hidden, rows_cot, across, preferred_element_type=jnp.float32
    ).astype(jnp.bfloat16)
    hidden_grad = lax.dot_general(rows_cot, w_down, inner, preferred_element_type=jnp.float32)
    gate_grad = (hidden_grad * up_act * squash * (1.0 + gate_act * (1.0 - squash))).astype(
        jnp.bfloat16
    )
    up_grad = (hidden_grad * silu_gate).astype(jnp.bfloat16)
    gate_w_grad = lax.dot_general(
        rows_in, gate_grad, across, preferred_element_type=jnp.float32
    ).astype(jnp.bfloat16)
    up_w_grad = lax.dot_general(
        rows_in, up_grad, across, preferred_element_type=jnp.float32
    ).astype(jnp.bfloat16)
    row_part = lax.dot_general(gate_grad, w_gate, inner, preferred_element_type=jnp.float32)
    row_part = row_part + lax.dot_general(up_grad, w_up, inner, preferred_element_type=jnp.float32)
    return (gate_w_grad, up_w_grad, down_grad, row_part)


def gather_back(returned, slot_index, cotangent, route_count):
    picked = jnp.take(returned, slot_index, axis=0).astype(jnp.float32)
    summed = jnp.sum(picked.reshape(-1, route_count, picked.shape[1]), axis=1)
    return (summed + cotangent.astype(jnp.float32)).astype(jnp.bfloat16)


def per_device(
    ffn_input,
    out_grad,
    routes,
    route_weight,
    gate_w,
    up_w,
    down_w,
    out_proj,
    rec_value,
    rate_pre,
    input_pre,
    prev_state,
    decay_param,
):
    experts = lax.axis_size(SP)
    tok_rows, route_count = routes.shape
    capacity = 5 * route_count * tok_rows // (4 * experts)
    slot_index, slot_owner, filled = slot_layout(routes, experts, capacity)
    w_gate, w_up, w_down = (gate_w[0], up_w[0], down_w[0])
    send_in, send_cot = fill_slots(
        ffn_input, out_grad, route_weight, slot_owner, filled, route_count
    )
    part_in, part_cot = in_one_piece((send_in, send_cot), SP, 0, 0, 1)
    got_in, got_cot = sent_together((part_in, part_cot), "tp", 1, 0)
    expert_out = expert_work(got_in, got_cot, w_gate, w_up, w_down)
    summed_share = sent_and_summed(expert_out[3].astype(jnp.bfloat16), "tp", 1).astype(jnp.bfloat16)
    returned = lax.all_to_all(summed_share, SP, split_axis=0, concat_axis=0, tiled=True)
    own_grad = gather_back(returned, slot_index, out_grad, route_count)
    mix_grad = lax.all_gather(own_grad, "tp", axis=1, tiled=True)
    state_grad = lax.dot_general(
        mix_grad, out_proj, (((1,), (1,)), ((), ())), preferred_element_type=jnp.float32
    )
    rate_gate = jax.nn.sigmoid(rate_pre.astype(jnp.float32))
    input_gate = jax.nn.sigmoid(input_pre.astype(jnp.float32))
    decay_speed = jax.nn.softplus(-decay_param)[None, :]
    log_decay = -decay_scale * rate_gate * decay_speed
    decay = jnp.exp(log_decay)
    scale_in = jnp.sqrt(-jnp.expm1(2.0 * log_decay))
    signal = rec_value.astype(jnp.float32)
    before_state = prev_state.astype(jnp.float32)
    rec_state = (decay * before_state + scale_in * input_gate * signal).astype(jnp.bfloat16)
    out_proj_grad = sent_and_summed(
        lax.dot_general(
            mix_grad, rec_state, (((0,), (0,)), ((), ())), preferred_element_type=jnp.float32
        ).astype(jnp.bfloat16),
        SP,
        0,
    )
    following = jnp.concatenate([decay[1:], jnp.ones_like(decay[:1])], axis=0)
    through, local_grad = lax.associative_scan(
        chain_link, (following[::-1], state_grad[::-1]), axis=0
    )
    through = through[::-1]
    local_grad = local_grad[::-1]
    chain_mult = decay[0] * through[0]
    chain_add = decay[0] * local_grad[0]
    _, incoming = entering(
        (chain_mult, chain_add), SP, compose, (jnp.ones_like(chain_mult), jnp.zeros_like(chain_add))
    )
    carried = local_grad + through * incoming[None, :]
    rec_value_grad = (carried * scale_in * input_gate).astype(jnp.bfloat16)
    input_pre_grad = (carried * scale_in * signal * input_gate * (1.0 - input_gate)).astype(
        jnp.bfloat16
    )
    decay_part = decay * before_state - input_gate * signal * decay * decay / scale_in
    rate_pre_grad = (
        carried * decay_part * (-decay_scale * decay_speed) * rate_gate * (1.0 - rate_gate)
    ).astype(jnp.bfloat16)
    return (
        expert_out[0][None],
        expert_out[1][None],
        expert_out[2][None],
        out_proj_grad,
        rec_value_grad,
        rate_pre_grad,
        input_pre_grad,
    )


def solution(mesh):
    finer = Mesh(mesh.devices.reshape(8, 4, mesh.shape["tp"]), ("sp_0", "sp_1", "tp"))
    placed = (
        P(SP, "tp"),
        P(SP, "tp"),
        P(SP, None),
        P(SP, None),
        P(SP, None, "tp"),
        P(SP, None, "tp"),
        P(SP, "tp", None),
        P("tp", None),
        P(SP, "tp"),
        P(SP, "tp"),
        P(SP, "tp"),
        P(SP, "tp"),
        P("tp"),
    )
    return jax.shard_map(
        per_device,
        mesh=finer,
        in_specs=placed,
        out_specs=(
            P(SP, None, "tp"),
            P(SP, None, "tp"),
            P(SP, "tp", None),
            P(SP, "tp"),
            P(SP, "tp"),
            P(SP, "tp"),
            P(SP, "tp"),
        ),
        check_vma=False,
    )
```

profile of v0, /device:TPU:8, one launch (start us, length us, event | category | flops | bytes accessed | tf_op | source)
XLA Modules:
  0.0 212.8 jit_solution(11607616895338328449)
XLA Ops:
  7.2 0.7 broadcast_multiply_fusion
  8.0 0.8 copy.33
  9.3 0.6 reduce-window.6
  10.2 1.4 scatter_custom_fusion.1
  11.7 1.4 scatter_custom_fusion
  13.1 1.9 gather_fusion.2
  15.0 1.9 gather_fusion.3
  16.9 0.8 copy.36
  17.8 2.5 %gather_fusion = f32[320]{0:T(512)S(1)} fusion(f32[256]{0:T(256)S(1)} %reshape.413, s32[1024]{0:T(1024)S(1)} %pad_clamp_fusion.1), kind=kCustom, calls=%fused_computation.2 | custom fusion | bytes 3840 | tf_op jit(solution)/shard_map/gather | solution.py:113
  20.6 25.8 %all_to_all.34 = bf16[32,10,256]{2,1,0:T(8,128)(2,1)S(1)} all-to-all(bf16[32,10,256]{2,1,0:T(8,128)(2,1)S(1)} %all_to_all.22), channel_id=1, replica_groups=mesh['sp_0'=8,'sp_1'=4,'tp'=16] {'sp_0','sp_1'}, dimensions={0} | all-to-all | bytes 327680 | tf_op jit(solution)/shard_map/all_to_all | solution.py:16
  46.5 0.7 pad_maximum_fusion.1
  47.2 40.4 %all-gather.6.cloned.1.call-done = bf16[640,2048]{1,0:T(8,128)(2,1)} async-done(((bf16[640,128]{1,0:T(8,128)(2,1)}), bf16[640,2048]{1,0:T(8,128)(2,1)}) %all-gather.6.cloned.1.call-update) | async-done | bytes 2621456 | tf_op jit(solution)/shard_map/all_gather | solution.py:32
  87.6 2.0 fusion.10
  89.6 1.8 fusion.12
  92.5 0.5 fusion.4
  93.0 1.4 copy.44
  94.4 5.6 %all-to-all-start.1 = ((bf16[16,320,128]{2,1,0:T(8,128)(2,1)}), bf16[16,320,128]{2,1,0:T(8,128)(2,1)S(1)}, u32[]{:S(2)}, u32[]{:S(2)}) async-start(bf16[16,320,128]{2,1,0:T(8,128)(2,1)} %bitcast.161), calls=%async_computation.1 | async-start | bytes 2621440 | tf_op jit(solution)/shard_map/all_to_all | solution.py:43
  100.6 2.7 %fusion.1 = bf16[1,2048,128]{2,1,0:T(8,128)(2,1)} fusion(bf16[320,128]{1,0:T(8,128)(2,1)S(1)} %get-tuple-element.11, bf16[640,2048]{1,0:T(8,128)(2,1)} %all-gather.6.cloned.1.call-done), kind=kOutput, calls=%fused_computation.12 | convolution fusion | flops 168034304 | bytes 1916928 | tf_op jit(solution)/shard_map/dot_general | solution.py:137
  103.4 2.6 %fusion.3 = bf16[1,128,2048]{2,1,0:T(8,128)(2,1)} fusion(bf16[640,2048]{1,0:T(8,128)(2,1)} %all-gather.6.cloned.1.call-done, f32[320,128]{1,0:T(8,128)S(1)} %fusion.12, f32[320,128]{1,0:T(8,128)S(1)} %fusion.10), kind=kOutput, calls=%fused_computation.14 | convolution fusion | flops 168280064 | bytes 2162688 | tf_op jit(solution)/shard_map/dot_general | solution.py:129
  106.0 24.2 %all-to-all-done.1 = bf16[16,320,128]{2,1,0:T(8,128)(2,1)S(1)} async-done(((bf16[16,320,128]{2,1,0:T(8,128)(2,1)}), bf16[16,320,128]{2,1,0:T(8,128)(2,1)S(1)}, u32[]{:S(2)}, u32[]{:S(2)}) %all-to-all-start.1) | async-done | bytes 1310752 | tf_op jit(solution)/shard_map/all_to_all | solution.py:43
  130.4 0.7 all_to_all.26
  131.1 10.2 %all-to-all-start.2 = ((bf16[32,10,128]{2,1,0:T(8,128)(2,1)}), bf16[32,10,128]{2,1,0:T(8,128)(2,1)S(1)}, u32[]{:S(2)}, u32[]{:S(2)}) async-start(bf16[32,10,128]{2,1,0:T(8,128)(2,1)} %all_to_all.26), calls=%async_computation.2 | async-start | bytes 262144 | tf_op jit(solution)/shard_map/all_to_all | solution.py:181
  141.3 2.8 %fusion.2 = bf16[1,2048,128]{2,1,0:T(8,128)(2,1)} fusion(bf16[320,128]{1,0:T(8,128)(2,1)S(1)} %get-tuple-element.10, bf16[640,2048]{1,0:T(8,128)(2,1)} %all-gather.6.cloned.1.call-done), kind=kOutput, calls=%fused_computation.13 | convolution fusion | flops 168034304 | bytes 1916928 | tf_op jit(solution)/shard_map/dot_general | solution.py:140
  144.0 8.2 %all-to-all-done.2 = bf16[32,10,128]{2,1,0:T(8,128)(2,1)S(1)} async-done(((bf16[32,10,128]{2,1,0:T(8,128)(2,1)}), bf16[32,10,128]{2,1,0:T(8,128)(2,1)S(1)}, u32[]{:S(2)}, u32[]{:S(2)}) %all-to-all-start.2) | async-done | bytes 81952 | tf_op jit(solution)/shard_map/all_to_all | solution.py:181
  152.3 0.9 gather_fusion.1
  153.4 17.8 %all_gather.19 = bf16[128,2048]{1,0:T(8,128)(2,1)S(1)} all-gather(bf16[128,128]{1,0:T(8,128)(2,1)S(1)} %add_convert_fusion), channel_id=1, replica_groups=mesh['sp_0'=8,'sp_1'=4,'tp'=16] {'tp'}, dimensions={1}, use_global_device_ids=true | all-gather | bytes 557056 | tf_op jit(solution)/shard_map/all_gather | solution.py:183
  172.4 1.2 convolution_convert_fusion
  173.6 3.9 %all-to-all-start.3 = ((bf16[32,64,128]{2,1,0:T(8,128)(2,1)}), bf16[32,64,128]{2,1,0:T(8,128)(2,1)S(1)}, u32[]{:S(2)}, u32[]{:S(2)}) async-start(bf16[32,64,128]{2,1,0:T(8,128)(2,1)} %bitcast.11), calls=%async_computation.3 | async-start | bytes 1048576 | tf_op jit(solution)/shard_map/all_to_all | solution.py:43
  178.3 9.9 %all-gather.2 = f32[4,2,128]{2,1,0:T(2,128)S(1)} all-gather(f32[1,2,128]{2,1,0:T(2,128)S(1)} %maximum_bitcast_fusion), channel_id=2, replica_groups=mesh['sp_0'=8,'sp_1'=4,'tp'=16] {'sp_1'}, dimensions={0}, use_global_device_ids=true | all-gather | bytes 5120 | tf_op jit(solution)/shard_map/all_gather | solution.py:61
  188.3 16.2 %all-gather.3 = f32[8,2,128]{2,1,0:T(2,128)S(1)} all-gather(f32[1,2,128]{2,1,0:T(2,128)S(1)} %maximum_bitcast_fusion.1), channel_id=3, replica_groups=mesh['sp_0'=8,'sp_1'=4,'tp'=16] {'sp_0'}, dimensions={0}, use_global_device_ids=true | all-gather | bytes 9216 | tf_op jit(solution)/shard_map/all_gather | solution.py:61
  204.5 0.8 fusion.26
  205.2 0.7 convert_reduce_fusion
  (184 shorter events, 5.0 us)
Async XLA Ops:
  7.2 80.4 %copy-start = (bf16[1,2048,128]{2,1,0:T(8,128)(2,1)S(1)}, bf16[1,2048,128]{2,1,0:T(8,128)(2,1)}, u32[]{:S(2)}) copy-start(bf16[1,2048,128]{2,1,0:T(8,128)(2,1)} %param.19) | copy-start | bytes 1572868
  7.2 80.4 %all-gather.6.cloned.1.call-start = ((), (), s32[]{:S(2)}) async-start(), calls=%async_computation.4 | async-start | bytes 2785280 | tf_op jit(solution)/shard_map/all_gather | solution.py:32
  20.3 69.3 %copy-start.3 = (bf16[1,2048,128]{2,1,0:T(8,128)(2,1)S(1)}, bf16[1,2048,128]{2,1,0:T(8,128)(2,1)}, u32[]{:S(2)}) copy-start(bf16[1,2048,128]{2,1,0:T(8,128)(2,1)} %param.20) | copy-start | bytes 1572868
  46.5 44.9 %copy-start.10 = (bf16[1,128,2048]{2,1,0:T(8,128)(2,1)S(1)}, bf16[1,128,2048]{2,1,0:T(8,128)(2,1)}, u32[]{:S(2)}) copy-start(bf16[1,128,2048]{2,1,0:T(8,128)(2,1)} %param.21) | copy-start | bytes 1572868
  87.6 3.8 %copy-start.2 = (bf16[640,2048]{1,0:T(8,128)(2,1)S(1)}, bf16[640,2048]{1,0:T(8,128)(2,1)}, u32[]{:S(2)}) copy-start(bf16[640,2048]{1,0:T(8,128)(2,1)} %all-gather.6.cloned.1.call-done) | copy-start | bytes 7864324
  93.0 7.2 %copy-start.11 = (f32[128]{0:T(128)S(1)}, f32[128]{0:T(128)}, u32[]{:S(2)}) copy-start(f32[128]{0:T(128)} %param.27) | copy-start | bytes 1540
  93.0 7.2 %copy-start.5 = (bf16[128,128]{1,0:T(8,128)(2,1)S(1)}, bf16[128,128]{1,0:T(8,128)(2,1)}, u32[]{:S(2)}) copy-start(bf16[128,128]{1,0:T(8,128)(2,1)} %param.24) | copy-start | bytes 98308
  93.0 7.4 %copy-start.9 = (s32[128,2]{0,1:T(2,128)S(1)}, s32[128,2]{0,1:T(2,128)}, u32[]{:S(2)}) copy-start(s32[128,2]{0,1:T(2,128)} %param.17) | copy-start | bytes 3076
  94.4 35.8 %all-to-all-start.1 = ((bf16[16,320,128]{2,1,0:T(8,128)(2,1)}), bf16[16,320,128]{2,1,0:T(8,128)(2,1)S(1)}, u32[]{:S(2)}, u32[]{:S(2)}) async-start(bf16[16,320,128]{2,1,0:T(8,128)(2,1)} %bitcast.161), calls=%async_computation.1 | async-start | bytes 2621440 | tf_op jit(solution)/shard_map/all_to_all | solution.py:43
  106.0 47.4 %copy-start.1 = (bf16[128,128]{1,0:T(8,128)(2,1)S(1)}, bf16[128,128]{1,0:T(8,128)(2,1)}, u32[]{:S(2)}) copy-start(bf16[128,128]{1,0:T(8,128)(2,1)} %param.16) | copy-start | bytes 98308
  106.0 65.3 %copy-start.4 = (bf16[128,2048]{1,0:T(8,128)(2,1)S(1)}, bf16[128,2048]{1,0:T(8,128)(2,1)}, u32[]{:S(2)}) copy-start(bf16[128,2048]{1,0:T(8,128)(2,1)} %param.22) | copy-start | bytes 1572868
  131.1 21.2 %all-to-all-start.2 = ((bf16[32,10,128]{2,1,0:T(8,128)(2,1)}), bf16[32,10,128]{2,1,0:T(8,128)(2,1)S(1)}, u32[]{:S(2)}, u32[]{:S(2)}) async-start(bf16[32,10,128]{2,1,0:T(8,128)(2,1)} %all_to_all.26), calls=%async_computation.2 | async-start | bytes 262144 | tf_op jit(solution)/shard_map/all_to_all | solution.py:181
  141.2 31.1 %copy-start.6 = (bf16[128,128]{1,0:T(8,128)(2,1)S(1)}, bf16[128,128]{1,0:T(8,128)(2,1)}, u32[]{:S(2)}) copy-start(bf16[128,128]{1,0:T(8,128)(2,1)} %param.23) | copy-start | bytes 98308
  141.2 31.1 %copy-start.7 = (bf16[128,128]{1,0:T(8,128)(2,1)S(1)}, bf16[128,128]{1,0:T(8,128)(2,1)}, u32[]{:S(2)}) copy-start(bf16[128,128]{1,0:T(8,128)(2,1)} %param.26) | copy-start | bytes 98308
  141.3 31.1 %copy-start.8 = (bf16[128,128]{1,0:T(8,128)(2,1)S(1)}, bf16[128,128]{1,0:T(8,128)(2,1)}, u32[]{:S(2)}) copy-start(bf16[128,128]{1,0:T(8,128)(2,1)} %param.25) | copy-start | bytes 98308
  173.6 31.6 %all-to-all-start.3 = ((bf16[32,64,128]{2,1,0:T(8,128)(2,1)}), bf16[32,64,128]{2,1,0:T(8,128)(2,1)S(1)}, u32[]{:S(2)}, u32[]{:S(2)}) async-start(bf16[32,64,128]{2,1,0:T(8,128)(2,1)} %bitcast.11), calls=%async_computation.3 | async-start | bytes 1048576 | tf_op jit(solution)/shard_map/all_to_all | solution.py:43
Sparse Core Ops, SparseCore 0:
  47.3 40.2 all-gather.5
where the time goes:
time: 213 us
  waiting for transfers between devices  72.8 us (34%)
  blocking collectives  69.7 us (33%)
  starting transfers between devices  19.7 us (9%)
  local copies, waits for them, and re-layouts  15.8 us (7%)
  between operations  15.1 us (7%)
  matrix products  14.9 us (7%)
  other arithmetic  4.78 us (2%)
    all_gather x1, waiting for transfers between devices, sent_together(): lax.all_gather(both, axis, axis=dim, tiled=True)  40.4 us
    all_gather x2, blocking collectives, all_in_one(): both, at, found = (lax.all_gather(jnp.concatenate(lines), axis), 0, {})  26.1 us
    all_to_all x1, blocking collectives, in_one_piece(): lax.all_to_all(both, axis, split_axis=split_dim, concat_axis=concat_dim,...  25.8 us
    all_to_all x2, waiting for transfers between devices, sent_and_summed(): lax.all_to_all(tiles, axis, split_axis=0, concat_axis=0, tiled=True)  24.2 us
    all_gather x1, blocking collectives, per_device(): mix_grad = lax.all_gather(own_grad, 'tp', axis=1, tiled=True)  17.8 us
    all_to_all x1, starting transfers between devices, per_device(): lax.all_to_all(summed_share, SP, split_axis=0, concat_axis=0, tiled=True)  10.2 us
    all_to_all x2, starting transfers between devices, sent_and_summed(): lax.all_to_all(tiles, axis, split_axis=0, concat_axis=0, tiled=True)  9.46 us
    all_to_all x1, waiting for transfers between devices, per_device(): lax.all_to_all(summed_share, SP, split_axis=0, concat_axis=0, tiled=True)  8.21 us
  transfers between devices with their start and end apart: 4, of which 3 were waited for; matrix products, arithmetic and copies ran while one was open for 5% of the time, Pallas kernels for 0%

commit v1 on v0

v1 whole, which is shorter than its diff:
```python
import functools

import jax
import jax.numpy as jnp
from jax import lax
from jax.experimental import pallas as pl
from jax.experimental.pallas import tpu as pltpu
from jax.sharding import Mesh
from jax.sharding import PartitionSpec as P

SP = ("z", "x")
TP = ("y", "c")
F32 = jnp.float32
BF16 = jnp.bfloat16
decay_scale = 8.0
PAD = 16


def whole(shape, dtype):
    return jax.ShapeDtypeStruct(shape, dtype)


def dot(a, b, dims):
    return lax.dot_general(a, b, (dims, ((), ())), preferred_element_type=F32)


def expert_body(got, wg, wu, wd, gu_grad, hidden, part):
    n_c, n_y, two_rows, fw = got.shape
    rows = two_rows // 2
    hid = wg.shape[1]
    acc = jnp.zeros((rows, 2 * hid), F32)
    back = jnp.zeros((rows, hid), F32)
    for y in range(n_y):
        at = pl.ds(y * n_c * fw, n_c * fw)
        x_in = jnp.concatenate([got[c, y, :rows, :] for c in range(n_c)], axis=1)
        x_cot = jnp.concatenate([got[c, y, rows:, :] for c in range(n_c)], axis=1)
        w_both = jnp.concatenate([wg[at, :], wu[at, :]], axis=1)
        acc = acc + dot(x_in, w_both, ((1,), (0,)))
        back = back + dot(x_cot, wd[:, at], ((1,), (1,)))
    gate, up = acc[:, :hid], acc[:, hid:]
    squash = jax.nn.sigmoid(gate)
    silu = gate * squash
    hidden[...] = (silu * up).astype(BF16)
    g_grad = (back * up * squash * (1.0 + gate * (1.0 - squash))).astype(BF16)
    u_grad = (back * silu).astype(BF16)
    both = jnp.concatenate([g_grad, u_grad], axis=1)
    gu_grad[...] = both
    for y in range(n_y):
        at = pl.ds(y * n_c * fw, n_c * fw)
        w_both = jnp.concatenate([wg[at, :], wu[at, :]], axis=1)
        r = dot(both, w_both, ((1,), (1,))).astype(BF16)
        for c in range(n_c):
            part[c, y] = r[:, c * fw : (c + 1) * fw]


def expert_rows_grad(got, wg, wu, wd):
    n_c, n_y, two_rows, fw = got.shape
    rows, hid = two_rows // 2, wg.shape[1]
    return pl.pallas_call(
        expert_body,
        out_shape=(
            whole((rows, 2 * hid), BF16),
            whole((rows, hid), BF16),
            whole((n_c, n_y, rows, fw), BF16),
        ),
        name="expert_rows_grad",
    )(got, wg, wu, wd)


def weight_body(got, gu_grad, hidden, dg, du, dd):
    n_c, n_y, two_rows, fw = got.shape
    rows = two_rows // 2
    hid = hidden.shape[1]
    for y in range(n_y):
        at = pl.ds(y * n_c * fw, n_c * fw)
        x_in = jnp.concatenate([got[c, y, :rows, :] for c in range(n_c)], axis=1)
        x_cot = jnp.concatenate([got[c, y, rows:, :] for c in range(n_c)], axis=1)
        both = dot(x_in, gu_grad[...], ((0,), (0,))).astype(BF16)
        dg[at, :] = both[:, :hid]
        du[at, :] = both[:, hid:]
        dd[:, at] = dot(hidden[...], x_cot, ((0,), (0,))).astype(BF16)


def expert_weight_grads(got, gu_grad, hidden):
    n_c, n_y, _, fw = got.shape
    d, hid = n_c * n_y * fw, hidden.shape[1]
    return pl.pallas_call(
        weight_body,
        out_shape=(whole((d, hid), BF16), whole((d, hid), BF16), whole((hid, d), BF16)),
        name="expert_weight_grads",
    )(got, gu_grad, hidden)


def slot_marks(routes, experts):
    tokens, count = routes.shape
    names = routes.T
    here = [names[k][None, :] == jnp.arange(experts, dtype=jnp.int32)[:, None] for k in range(count)]
    named = functools.reduce(jnp.logical_or, here).astype(BF16)
    t = jnp.arange(tokens, dtype=jnp.int32)
    earlier = (t[:, None] < t[None, :]).astype(BF16)
    before = dot(named, earlier, ((1,), (0,)))
    row = jnp.arange(experts * PAD, dtype=jnp.int32)[:, None]
    marks = []
    for k in range(count):
        rank = jnp.sum(jnp.where(here[k], before, 0.0), axis=0).astype(jnp.int32)
        marks.append(row == (names[k] * PAD + rank)[None, :])
    return marks


def chain_link(left_pair, right_pair):
    return (left_pair[0] * right_pair[0], right_pair[0] * left_pair[1] + right_pair[1])


def in_three(v):
    hi = lax.reduce_precision(v, 8, 7)
    mid = lax.reduce_precision(v - hi, 8, 7)
    return [p.astype(BF16) for p in (hi, mid, v - hi - mid)]


def of_three(a):
    return (a[2].astype(F32) + a[1].astype(F32)) + a[0].astype(F32)


def per_device(
    ffn_input,
    out_grad,
    routes,
    route_weight,
    gate_w,
    up_w,
    down_w,
    out_proj,
    rec_value,
    rate_pre,
    input_pre,
    prev_state,
    decay_param,
):
    n_sp, n_y, n_c = lax.axis_size(SP), lax.axis_size("y"), lax.axis_size("c")
    tok, count = routes.shape
    cap = 5 * count * tok // (4 * n_sp)
    rows = n_sp * cap
    fw = ffn_input.shape[1]

    marks = slot_marks(routes, n_sp)
    pick = functools.reduce(jnp.logical_or, marks).astype(BF16)
    weight = sum(jnp.sum(jnp.where(m, route_weight.T[k][None, :], 0.0), axis=1) for k, m in enumerate(marks))
    rows_in = dot(pick, ffn_input, ((1,), (0,))).astype(BF16)
    rows_cot = (weight[:, None] * dot(pick, out_grad, ((1,), (0,)))).astype(BF16)
    send = jnp.concatenate([rows_in, rows_cot], axis=1).reshape(n_sp, PAD, 2 * fw)
    recv = lax.all_to_all(send, SP, 0, 0, tiled=True)[:, :cap]
    own = jnp.concatenate(
        [recv[:, :, :fw].reshape(rows, fw), recv[:, :, fw:].reshape(rows, fw)], axis=0
    )
    over_y = lax.all_to_all(
        jnp.broadcast_to(own[None], (n_y, 2 * rows, fw)), "y", 0, 0, tiled=True
    )
    got = lax.all_to_all(
        jnp.broadcast_to(over_y[None], (n_c, n_y, 2 * rows, fw)), "c", 0, 0, tiled=True
    )

    gu_grad, hidden, part = expert_rows_grad(got, gate_w[0], up_w[0], down_w[0])
    chip = lax.all_to_all(part, "c", 0, 0, tiled=True).astype(F32).sum(axis=0).astype(BF16)
    share = lax.all_to_all(chip, "y", 0, 0, tiled=True).astype(F32).sum(axis=0).astype(BF16)
    d_gate, d_up, d_down = expert_weight_grads(got, gu_grad, hidden)

    back = jnp.pad(share.reshape(n_sp, cap, fw), ((0, 0), (0, PAD - cap), (0, 0)))
    returned = lax.all_to_all(back, SP, 0, 0, tiled=True).reshape(n_sp * PAD, fw)
    own_grad = (dot(pick, returned, ((0,), (0,))) + out_grad.astype(F32)).astype(BF16)
    mix_grad = lax.all_gather(own_grad, TP, axis=1, tiled=True)

    rate_gate = jax.nn.sigmoid(rate_pre.astype(F32))
    input_gate = jax.nn.sigmoid(input_pre.astype(F32))
    decay_speed = jax.nn.softplus(-decay_param)[None, :]
    log_decay = -decay_scale * rate_gate * decay_speed
    decay = jnp.exp(log_decay)
    scale_in = jnp.sqrt(-jnp.expm1(2.0 * log_decay))
    signal = rec_value.astype(F32)
    before_state = prev_state.astype(F32)
    rec_state = (decay * before_state + scale_in * input_gate * signal).astype(BF16)
    following = jnp.concatenate([decay[1:], jnp.ones_like(decay[:1])], axis=0)

    state_grad = dot(mix_grad, out_proj, ((1,), (1,)))
    through, local_grad = lax.associative_scan(chain_link, (following, state_grad), axis=0, reverse=True)
    proj_part = dot(mix_grad, rec_state, ((0,), (0,))).astype(BF16)
    chain = in_three(decay[0] * through[0]) + in_three(decay[0] * local_grad[0])
    chain = jnp.pad(jnp.stack(chain), ((0, 8 - len(chain)), (0, 0)))
    width = proj_part.shape[1]
    last = jnp.concatenate(
        [
            proj_part.reshape(n_sp, -1, width),
            jnp.broadcast_to(chain[None], (n_sp, *chain.shape)),
        ],
        axis=1,
    )
    last = lax.all_to_all(last, SP, 0, 0, tiled=True)
    keep = proj_part.shape[0] // n_sp
    out_proj_grad = last[:, :keep].astype(F32).sum(axis=0)
    mult = of_three([last[:, keep + i] for i in range(3)])
    add = of_three([last[:, keep + 3 + i] for i in range(3)])
    here = lax.axis_index(SP)
    incoming = jnp.zeros_like(add[0])
    for k in reversed(range(n_sp)):
        incoming = jnp.where(k > here, add[k] + mult[k] * incoming, incoming)
    carried = local_grad + through * incoming[None, :]

    rec_value_grad = (carried * scale_in * input_gate).astype(BF16)
    input_pre_grad = (carried * scale_in * signal * input_gate * (1.0 - input_gate)).astype(BF16)
    decay_part = decay * before_state - input_gate * signal * decay * decay / scale_in
    rate_pre_grad = (
        carried * decay_part * (-decay_scale * decay_speed) * rate_gate * (1.0 - rate_gate)
    ).astype(BF16)
    return (
        d_gate[None],
        d_up[None],
        d_down[None],
        out_proj_grad,
        rec_value_grad,
        rate_pre_grad,
        input_pre_grad,
    )


def solution(mesh):
    finer = Mesh(mesh.devices.reshape(8, 4, 8, 2), ("z", "x", "y", "c"))
    grid = P(SP, TP)
    return jax.shard_map(
        per_device,
        mesh=finer,
        in_specs=(
            grid,
            grid,
            P(SP, None),
            P(SP, None),
            P(SP, None, TP),
            P(SP, None, TP),
            P(SP, TP, None),
            P(TP, None),
            grid,
            grid,
            grid,
            grid,
            P(TP),
        ),
        out_specs=(P(SP, None, TP), P(SP, None, TP), P(SP, TP, None), grid, grid, grid, grid),
        check_vma=False,
    )
```

time: 213 us -> 174 us (0.82)
  blocking collectives: 69.7 us -> 117 us
  waiting for transfers between devices: 72.8 us -> 25.8 us
  between operations: 15.1 us -> 1.54 us
  matrix products: 14.9 us -> 3.07 us
  local copies, waits for them, and re-layouts: 15.8 us -> 4.1 us
  starting transfers between devices: 19.7 us -> 8.87 us
  Pallas kernels: 0 us -> 8.48 us
    all_to_all x1 -> x5, blocking collectives: 25.8 us -> 100 us  [the longest x1 38.5 us: per_device(): lax.all_to_all(jnp.broadcast_to(own[None], (n_y, 2 * rows, fw)), 'y', 0,...]
    all_gather x1 -> x0, waiting for transfers between devices: 40.4 us -> none  [sent_together(): lax.all_gather(both, axis, axis=dim, tiled=True)]
    all_gather x3 -> x1, blocking collectives: 43.9 us -> 17 us  [per_device(): mix_grad = lax.all_gather(own_grad, TP, axis=1, tiled=True)]
    dot_general x10 -> x6, matrix products: 14.9 us -> 3.07 us  [dot(): return lax.dot_general(a, b, (dims, ((), ())), preferred_element_type=F32)]
    all_to_all x3 -> x2, starting transfers between devices: 19.6 us -> 8.87 us  [the longest x1 4.98 us: per_device(): lax.all_to_all(back, SP, 0, 0, tiled=True).reshape(n_sp * PAD, fw)]
    pallas_call x0 -> x2, Pallas kernels: none -> 8.48 us  [the longest x1 4.47 us: expert_rows_grad(): pl.pallas_call(expert_body, out_shape=(whole((rows, 2 * hid), BF16), whol...]
    gather x4 -> x0, local copies, waits for them, and re-layouts: 7.09 us -> none  [the longest x1 2.46 us: fill_slots(): weights = route_weight.reshape(-1)[slot_owner][:, None]]
    all_to_all x3 -> x2, waiting for transfers between devices: 32.4 us -> 25.8 us  [the longest x1 15.4 us: per_device(): last = lax.all_to_all(last, SP, 0, 0, tiled=True)]
  transfers between devices with their start and end apart: 4 -> 2, of which waited for: 3 -> 2; matrix products, arithmetic and copies ran while one was open for 5% -> 0% of each run, Pallas kernels for 0% -> 2%
where the time goes in v1:
time: 174 us
  blocking collectives  117 us (67%)
  waiting for transfers between devices  25.8 us (15%)
  starting transfers between devices  8.87 us (5%)
  Pallas kernels  8.48 us (5%)
  other arithmetic  4.53 us (3%)
  local copies, waits for them, and re-layouts  4.1 us (2%)
  matrix products  3.07 us (2%)
    all_to_all x1, blocking collectives, per_device(): lax.all_to_all(jnp.broadcast_to(own[None], (n_y, 2 * rows, fw)), 'y', 0,...  38.5 us
    all_to_all x1, blocking collectives, per_device(): recv = lax.all_to_all(send, SP, 0, 0, tiled=True)[:, :cap]  25.8 us
    all_to_all x1, blocking collectives, per_device(): lax.all_to_all(chip, 'y', 0, 0, tiled=True).astype(F32).sum(axis=0)  23.3 us
    all_gather x1, blocking collectives, per_device(): mix_grad = lax.all_gather(own_grad, TP, axis=1, tiled=True)  17 us
    all_to_all x1, waiting for transfers between devices, per_device(): last = lax.all_to_all(last, SP, 0, 0, tiled=True)  15.4 us
    all_to_all x1, waiting for transfers between devices, per_device(): lax.all_to_all(back, SP, 0, 0, tiled=True).reshape(n_sp * PAD, fw)  10.4 us
    all_to_all x1, blocking collectives, per_device(): lax.all_to_all(jnp.broadcast_to(over_y[None], (n_c, n_y, 2 * rows, fw)),...  6.77 us
    all_to_all x1, blocking collectives, per_device(): lax.all_to_all(part, 'c', 0, 0, tiled=True).astype(F32).sum(axis=0)  5.92 us
  transfers between devices with their start and end apart: 2, of which 2 were waited for; matrix products, arithmetic and copies ran while one was open for 0% of the time, Pallas kernels for 2%

profile of v1, /device:TPU:8, one launch (start us, length us, event | category | flops | bytes accessed | tf_op | source)
XLA Modules:
  0.0 173.6 jit_solution(11721255060822612425)
XLA Ops:
  0.6 0.8 slice_bitcast_fusion.65
  1.4 0.8 slice_bitcast_fusion.62
  2.2 0.2 select_reduce_fusion.2
  2.3 0.8 fusion.108
  3.1 1.0 convolution_convert_fusion.1
  4.1 0.2 select_reduce_fusion
  4.3 1.0 fusion
  5.3 0.1 copy.23
  5.4 25.8 %all_to_all.35 = bf16[32,16,256]{2,1,0:T(8,128)(2,1)S(1)} all-to-all(bf16[32,16,256]{2,1,0:T(8,128)(2,1)S(1)} %bitcast.599), channel_id=1, replica_groups=mesh['z'=8,'x'=4,'y'=8,'c'=2] {'z','x'}, dimensions={0} | all-to-all | bytes 524288 | tf_op jit(solution)/shard_map/all_to_all | solution.py:151
  31.4 0.2 broadcast_in_dim.72
  31.6 38.5 %all_to_all.36 = bf16[8,640,128]{2,1,0:T(8,128)(2,1)S(1)} all-to-all(bf16[8,640,128]{2,1,0:T(8,128)(2,1)S(1)} %broadcast_in_dim.72), channel_id=1, replica_groups=mesh['z'=8,'x'=4,'y'=8,'c'=2] {'y'}, dimensions={0} | all-to-all | bytes 2621440 | tf_op jit(solution)/shard_map/all_to_all | solution.py:155
  70.0 0.5 broadcast_in_dim.73
  70.5 6.8 %all_to_all.37.got = bf16[2,8,640,128]{3,2,1,0:T(8,128)(2,1)} all-to-all(bf16[2,8,640,128]{3,2,1,0:T(8,128)(2,1)S(1)} %broadcast_in_dim.73), channel_id=1, replica_groups=mesh['z'=8,'x'=4,'y'=8,'c'=2] {'c'}, dimensions={0} | all-to-all | bytes 5242880 | tf_op jit(solution)/shard_map/all_to_all | solution.py:158
  77.3 4.5 %expert_rows_grad.1 = (bf16[320,256]{1,0:T(8,128)(2,1)}, bf16[320,128]{1,0:T(8,128)(2,1)}, bf16[2,8,320,128]{3,2,1,0:T(8,128)(2,1)}) custom-call(bf16[2,8,640,128]{3,2,1,0:T(8,128)(2,1)} %all_to_all.37.got, bf16[2048,128]{1,0:T(8,128)(2,1)} %bitcast.601, bf16[2048,128]{1,0:T(8,128)(2,1)} %bitcast.602, bf16[128,2048]{1,0:T(8,128)(2,1)} %bitcast.603), custom_call_target="tpu_custom_call" | custom-call | tf_op jit(solution)/shard_map/expert_rows_grad/pallas_call | solution.py:59
  81.8 5.9 %all_to_all.38 = bf16[2,8,320,128]{3,2,1,0:T(8,128)(2,1)S(1)} all-to-all(bf16[2,8,320,128]{3,2,1,0:T(8,128)(2,1)} %get-tuple-element.18), channel_id=1, replica_groups=mesh['z'=8,'x'=4,'y'=8,'c'=2] {'c'}, dimensions={0} | all-to-all | bytes 2621440 | tf_op jit(solution)/shard_map/all_to_all | solution.py:163
  87.7 0.5 reduce_sum.73
  88.2 23.3 %all_to_all.39 = bf16[8,320,128]{2,1,0:T(8,128)(2,1)S(1)} all-to-all(bf16[8,320,128]{2,1,0:T(8,128)(2,1)S(1)} %reduce_sum.73), channel_id=1, replica_groups=mesh['z'=8,'x'=4,'y'=8,'c'=2] {'y'}, dimensions={0} | all-to-all | bytes 1310720 | tf_op jit(solution)/shard_map/all_to_all | solution.py:164
  111.5 0.1 reduce_sum.74
  111.7 0.7 pad.96
  112.3 5.0 %all-to-all-start.5 = ((bf16[32,16,128]{2,1,0:T(8,128)(2,1)}), bf16[32,16,128]{2,1,0:T(8,128)(2,1)S(1)}, u32[]{:S(2)}, u32[]{:S(2)}) async-start(bf16[32,16,128]{2,1,0:T(8,128)(2,1)} %pad.96), calls=%async_computation.5 | async-start | bytes 262144 | tf_op jit(solution)/shard_map/all_to_all | solution.py:168
  117.6 10.4 %all-to-all-done.5 = bf16[32,16,128]{2,1,0:T(8,128)(2,1)S(1)} async-done(((bf16[32,16,128]{2,1,0:T(8,128)(2,1)}), bf16[32,16,128]{2,1,0:T(8,128)(2,1)S(1)}, u32[]{:S(2)}, u32[]{:S(2)}) %all-to-all-start.5) | async-done | bytes 131104 | tf_op jit(solution)/shard_map/all_to_all | solution.py:168
  128.0 0.3 fusion.1
  128.2 17.0 %all_gather.3 = bf16[128,2048]{1,0:T(8,128)(2,1)S(1)} all-gather(bf16[128,128]{1,0:T(8,128)(2,1)S(1)} %fusion.1), channel_id=1, replica_groups=mesh['z'=8,'x'=4,'y'=8,'c'=2] {'y','c'}, dimensions={1}, use_global_device_ids=true | all-gather | bytes 557056 | tf_op jit(solution)/shard_map/all_gather | solution.py:170
  145.3 0.3 fusion.113
  147.2 0.4 convolution_convert_fusion
  147.7 0.9 pad_maximum_fusion
  148.5 3.9 %all-to-all-start.6 = ((bf16[32,72,128]{2,1,0:T(8,128)(2,1)}), bf16[32,72,128]{2,1,0:T(8,128)(2,1)S(1)}, u32[]{:S(2)}, u32[]{:S(2)}) async-start(bf16[32,72,128]{2,1,0:T(8,128)(2,1)} %pad_maximum_fusion), calls=%async_computation.6 | async-start | bytes 1179648 | tf_op jit(solution)/shard_map/all_to_all | solution.py:196
  152.5 4.0 %expert_weight_grads.1 = (bf16[2048,128]{1,0:T(8,128)(2,1)}, bf16[2048,128]{1,0:T(8,128)(2,1)}, bf16[128,2048]{1,0:T(8,128)(2,1)}) custom-call(bf16[2,8,640,128]{3,2,1,0:T(8,128)(2,1)} %all_to_all.37.got, bf16[320,256]{1,0:T(8,128)(2,1)} %get-tuple-element.13.gu_grad, bf16[320,128]{1,0:T(8,128)(2,1)} %get-tuple-element.14.hidden), custom_call_target="tpu_custom_call" | custom-call | tf_op jit(solution)/shard_map/expert_weight_grads/pallas_call | solution.py:87
  156.6 15.4 %all-to-all-done.6 = bf16[32,72,128]{2,1,0:T(8,128)(2,1)S(1)} async-done(((bf16[32,72,128]{2,1,0:T(8,128)(2,1)}), bf16[32,72,128]{2,1,0:T(8,128)(2,1)S(1)}, u32[]{:S(2)}, u32[]{:S(2)}) %all-to-all-start.6) | async-done | bytes 589856 | tf_op jit(solution)/shard_map/all_to_all | solution.py:196
  172.0 0.1 fusion.42
  172.2 0.8 fusion.16
  172.9 0.7 convert_reduce_fusion
  (146 shorter events, 1.6 us)
Async XLA Ops:
  0.6 144.6 %copy-start = (bf16[128,2048]{1,0:T(8,128)(2,1)S(1)}, bf16[128,2048]{1,0:T(8,128)(2,1)}, u32[]{:S(2)}) copy-start(bf16[128,2048]{1,0:T(8,128)(2,1)} %param.20) | copy-start | bytes 1572868
  88.2 29.1 %copy-start.6 = (f32[128]{0:T(128)S(1)}, f32[128]{0:T(128)}, u32[]{:S(2)}) copy-start(f32[128]{0:T(128)} %param.25) | copy-start | bytes 1540
  88.2 29.1 %copy-start.1 = (bf16[128,128]{1,0:T(8,128)(2,1)S(1)}, bf16[128,128]{1,0:T(8,128)(2,1)}, u32[]{:S(2)}) copy-start(bf16[128,128]{1,0:T(8,128)(2,1)} %param.22) | copy-start | bytes 98308
  111.5 16.4 %copy-start.5 = (bf16[128,128]{1,0:T(8,128)(2,1)S(1)}, bf16[128,128]{1,0:T(8,128)(2,1)}, u32[]{:S(2)}) copy-start(bf16[128,128]{1,0:T(8,128)(2,1)} %param.14) | copy-start | bytes 98308
  112.3 15.6 %all-to-all-start.5 = ((bf16[32,16,128]{2,1,0:T(8,128)(2,1)}), bf16[32,16,128]{2,1,0:T(8,128)(2,1)S(1)}, u32[]{:S(2)}, u32[]{:S(2)}) async-start(bf16[32,16,128]{2,1,0:T(8,128)(2,1)} %pad.96), calls=%async_computation.5 | async-start | bytes 262144 | tf_op jit(solution)/shard_map/all_to_all | solution.py:168
  145.7 1.5 copy-start.2
  145.7 1.5 copy-start.3
  145.8 1.5 copy-start.4
  148.5 23.4 %all-to-all-start.6 = ((bf16[32,72,128]{2,1,0:T(8,128)(2,1)}), bf16[32,72,128]{2,1,0:T(8,128)(2,1)S(1)}, u32[]{:S(2)}, u32[]{:S(2)}) async-start(bf16[32,72,128]{2,1,0:T(8,128)(2,1)} %pad_maximum_fusion), calls=%async_computation.6 | async-start | bytes 1179648 | tf_op jit(solution)/shard_map/all_to_all | solution.py:196
